TPU v7x, 32 devices: a whole 2x2x4 slice. The times are simulated.
32 devices in a mesh: grp: 2 (over y), fs: 4 (over z), tp: 4 (over x, core).
Axes of the slice: x: 2, y: 2, z: 4, core: 2. Of those that a mesh axis runs over, the one named last changes fastest.
Arguments:
- tokens: bfloat16 [2048, 2048], P(('grp', 'fs'), 'tp'), parts along dimension 0, may hold values from -6 to 6
- recurrent_norm_gain: float32 [2048], replicated, may hold values from 0.1 to 1.9
- feedforward_norm_gain: float32 [2048], replicated, may hold values from 0.1 to 1.9
- gate_projection_weight: bfloat16 [2048, 2048], P('fs', 'tp'), may hold values from -0.125 to 0.125
- recurrent_projection_weight: bfloat16 [2048, 2048], P('fs', 'tp'), may hold values from -0.125 to 0.125
- convolution_kernel: bfloat16 [4, 2048], P(None, 'tp'), may hold values from -3 to 3
- decay_gate_matrix: bfloat16 [16, 128, 128], P('tp'), may hold values from -0.5 to 0.5
- input_gate_matrix: bfloat16 [16, 128, 128], P('tp'), may hold values from -0.5 to 0.5
- base_decay_logit: float32 [2048], P('tp'), may hold values from 3 to 9
- extra_log_decay: float32 [2048], P(('grp', 'fs')), parts along dimension 0, may hold values from -0.7 to 0
- output_projection_weight: bfloat16 [2048, 2048], P('tp', 'fs'), may hold values from -0.125 to 0.125
- up_projection_weight: bfloat16 [2048, 8192], P('fs', 'tp'), may hold values from -0.125 to 0.125
- down_projection_weight: bfloat16 [8192, 2048], P('tp', 'fs'), may hold values from -0.0625 to 0.0625
Outputs:
- layer_out: bfloat16 [2048, 2048], P(('grp', 'fs'), 'tp'), parts along dimension 0
There are 2 independent parts, one for each index of `grp`. A program takes and returns all parts, laid end to end along the dimension named above; an argument that names none is the same for every part. Nothing has to cross between parts.
All inputs are finite; a program needn't handle non-finite values.
Results may differ from a plain program's by a relative error of at most 0.018.
Values may be sent and summed in bfloat16 or wider, within the bound.
A program may use at most 64 MiB of HBM per device.

v0:
```python
import jax
import jax.numpy as jnp
from jax import lax
from jax.sharding import PartitionSpec as P


def rms_rows(values_in, norm_gain):
    values = values_in.astype(jnp.float32)
    inverse = lax.rsqrt(jnp.mean(values * values, axis=-1, keepdims=True) + 1e-06)
    return (values * inverse * norm_gain).astype(jnp.bfloat16)


def combine(earlier, later):
    return (earlier[0] * later[0], later[0] * earlier[1] + later[1])


def recurrent_state(
    recurrent_branch_rows,
    gate_branch_rows,
    convolution_kernel,
    decay_gate_matrix,
    input_gate_matrix,
    base_decay_logit,
    extra_log_decay,
):
    length = recurrent_branch_rows.shape[0]
    taps = convolution_kernel.shape[0]
    padded = jnp.pad(recurrent_branch_rows.astype(jnp.float32), ((taps - 1, 0), (0, 0)))
    conv_sum = jnp.zeros((length, recurrent_branch_rows.shape[1]), jnp.float32)
    for tap_index in range(taps):
        conv_sum = conv_sum + padded[tap_index : tap_index + length] * convolution_kernel[
            tap_index
        ].astype(jnp.float32)
    conv_rows = conv_sum.astype(jnp.bfloat16)
    blocks = decay_gate_matrix.shape[0]
    blocked = conv_rows.reshape(length, blocks, -1)
    recurrence_gate = jax.nn.sigmoid(
        jnp.einsum(
            "tni,nij->tnj", blocked, decay_gate_matrix, preferred_element_type=jnp.float32
        ).reshape(length, -1)
    )
    input_rate = jax.nn.sigmoid(
        jnp.einsum(
            "tni,nij->tnj", blocked, input_gate_matrix, preferred_element_type=jnp.float32
        ).reshape(length, -1)
    )
    decay_log_values = (
        -8.0 * jax.nn.softplus(-base_decay_logit) * recurrence_gate + extra_log_decay[:, None]
    )
    decay = jnp.exp(decay_log_values)
    drive = (
        jnp.sqrt(-jnp.expm1(2.0 * decay_log_values)) * input_rate * conv_rows.astype(jnp.float32)
    )
    _, hidden = lax.associative_scan(combine, (decay, drive), axis=0)
    return (hidden * gate_branch_rows.astype(jnp.float32)).astype(jnp.bfloat16)


def per_device(
    tokens,
    recurrent_norm_gain,
    feedforward_norm_gain,
    gate_projection_weight,
    recurrent_projection_weight,
    convolution_kernel,
    decay_gate_matrix,
    input_gate_matrix,
    base_decay_logit,
    extra_log_decay,
    output_projection_weight,
    up_projection_weight,
    down_projection_weight,
):
    whole_rows = lax.all_gather(tokens, "tp", axis=1, tiled=True)
    normed = rms_rows(whole_rows, recurrent_norm_gain)
    columns = normed
    gate_pre = jnp.dot(
        columns,
        lax.all_gather(gate_projection_weight, "fs", axis=0, tiled=True),
        preferred_element_type=jnp.float32,
    )
    recur_pre = jnp.dot(
        columns,
        lax.all_gather(recurrent_projection_weight, "fs", axis=0, tiled=True),
        preferred_element_type=jnp.float32,
    )
    gate_branch_rows = jax.nn.gelu(gate_pre).astype(jnp.bfloat16)
    recurrent_branch_rows = recur_pre.astype(jnp.bfloat16)
    mixed_output = recurrent_state(
        recurrent_branch_rows,
        gate_branch_rows,
        convolution_kernel,
        decay_gate_matrix,
        input_gate_matrix,
        base_decay_logit,
        extra_log_decay,
    )
    partials = jnp.dot(
        mixed_output,
        lax.all_gather(output_projection_weight, "fs", axis=1, tiled=True),
        preferred_element_type=jnp.float32,
    )
    residual = (
        tokens.astype(jnp.float32)
        + lax.psum_scatter(
            partials.astype(jnp.bfloat16), "tp", scatter_dimension=1, tiled=True
        ).astype(jnp.float32)
    ).astype(jnp.bfloat16)
    middle = lax.all_gather(residual, "tp", axis=1, tiled=True)
    channel_in = rms_rows(middle, feedforward_norm_gain)
    columns = channel_in
    upward = jnp.dot(
        columns,
        lax.all_gather(up_projection_weight, "fs", axis=0, tiled=True),
        preferred_element_type=jnp.float32,
    )
    positive = jnp.maximum(upward, 0.0)
    squared = (positive * positive).astype(jnp.bfloat16)
    down_terms = jnp.dot(
        squared,
        lax.all_gather(down_projection_weight, "fs", axis=1, tiled=True),
        preferred_element_type=jnp.float32,
    )
    summed_down = lax.psum_scatter(
        down_terms.astype(jnp.bfloat16), "tp", scatter_dimension=1, tiled=True
    ).astype(jnp.float32)
    return (residual.astype(jnp.float32) + summed_down).astype(jnp.bfloat16)


def solution(mesh):
    placed = (
        P(("grp", "fs"), "tp"),
        P(),
        P(),
        P("fs", "tp"),
        P("fs", "tp"),
        P(None, "tp"),
        P("tp", None, None),
        P("tp", None, None),
        P("tp"),
        P(("grp", "fs")),
        P("tp", "fs"),
        P("fs", "tp"),
        P("tp", "fs"),
    )
    return jax.shard_map(
        per_device, mesh=mesh, in_specs=placed, out_specs=P(("grp", "fs"), "tp"), check_vma=False
    )
```

profile of v0, /device:TPU:0, one launch (start us, length us, event | category | flops | bytes accessed | tf_op | source)
XLA Modules:
  0.0 558.3 jit_solution(17213416898491841167)
XLA Ops:
  6.5 0.7 all-gather.8.cloned.1.call-update
  7.3 0.7 all-gather.10.cloned.1.call-update
  8.1 0.7 all-gather.12.cloned.1.call-update
  9.4 0.8 slice_convert_fusion.3
  10.2 0.7 fusion.55
  10.9 17.4 %all-gather.8.cloned.1.call-done = bf16[256,2048]{1,0:T(8,128)(2,1)} async-done(((bf16[256,512]{1,0:T(8,128)(2,1)}), bf16[256,2048]{1,0:T(8,128)(2,1)}) %all-gather.8.cloned.1.call-update) | async-done | bytes 1048592 | tf_op jit(solution)/shard_map/all_gather | solution.py:73
  28.4 1.5 fusion.2
  29.9 45.7 %all-gather.10.cloned.1.call-done = bf16[2048,512]{1,0:T(8,128)(2,1)} async-done(((bf16[512,512]{1,0:T(8,128)(2,1)}), bf16[2048,512]{1,0:T(8,128)(2,1)}) %all-gather.10.cloned.1.call-update) | async-done | bytes 2097168 | tf_op jit(solution)/shard_map/all_gather | solution.py:83
  75.6 2.7 fusion.14
  79.8 0.7 fusion.29
  85.2 36.4 %all-gather.12.cloned.1.call-done = bf16[2048,512]{1,0:T(8,128)(2,1)} async-done(((bf16[512,512]{1,0:T(8,128)(2,1)}), bf16[2048,512]{1,0:T(8,128)(2,1)}) %all-gather.12.cloned.1.call-update) | async-done | bytes 2097168 | tf_op jit(solution)/shard_map/all_gather | solution.py:78
  121.7 45.9 %all-gather.14.cloned.1.call-done = bf16[512,2048]{1,0:T(8,128)(2,1)} async-done(((bf16[512,512]{1,0:T(8,128)(2,1)}), bf16[512,2048]{1,0:T(8,128)(2,1)}) %all-gather.14.cloned.1.call-update) | async-done | bytes 2097168 | tf_op jit(solution)/shard_map/all_gather | solution.py:99
  167.6 4.8 convolution_convert_fusion
  172.5 23.7 %reduce-scatter.3.cloned.1.call-done = bf16[256,512]{1,0:T(8,128)(2,1)} async-done(((bf16[256,2048]{1,0:T(8,128)(2,1)}), bf16[256,512]{1,0:T(8,128)(2,1)}) %reduce-scatter.3.cloned.1.call-update) | async-done | bytes 262160 | tf_op jit(solution)/shard_map/reduce_scatter | solution.py:104
  196.1 1.7 add_convert_fusion.1
  197.9 0.7 all-gather.18.cloned.1.call-update
  198.7 0.7 all-gather.20.cloned.1.call-update
  199.4 15.3 %all-gather.16.cloned.1.call-done = bf16[256,2048]{1,0:T(8,128)(2,1)} async-done(((bf16[256,512]{1,0:T(8,128)(2,1)}), bf16[256,2048]{1,0:T(8,128)(2,1)}) %all-gather.16.cloned.1.call-update) | async-done | bytes 1048592 | tf_op jit(solution)/shard_map/all_gather | solution.py:108
  214.7 1.5 fusion.5
  216.3 149.7 %all-gather.18.cloned.1.call-done = bf16[2048,2048]{1,0:T(8,128)(2,1)} async-done(((bf16[512,2048]{1,0:T(8,128)(2,1)}), bf16[2048,2048]{1,0:T(8,128)(2,1)}) %all-gather.18.cloned.1.call-update) | async-done | bytes 8388624 | tf_op jit(solution)/shard_map/all_gather | solution.py:113
  366.0 149.4 %all-gather.20.cloned.1.call-done = bf16[2048,2048]{1,0:T(8,128)(2,1)} async-done(((bf16[2048,512]{1,0:T(8,128)(2,1)}), bf16[2048,2048]{1,0:T(8,128)(2,1)}) %all-gather.20.cloned.1.call-update) | async-done | bytes 8388624 | tf_op jit(solution)/shard_map/all_gather | solution.py:120
  515.4 11.6 %convolution_convert_fusion.1 = bf16[256,2048]{1,0:T(8,128)(2,1)} fusion(bf16[2048,2048]{1,0:T(8,128)(2,1)} %all-gather.20.cloned.1.call-done, bf16[2048,2048]{1,0:T(8,128)(2,1)} %all-gather.18.cloned.1.call-done, bf16[256,2048]{1,0:T(8,128)(2,1)} %all-gather.16.cloned.1.call-done, f32[2048]{0:T(1024)S(1)} %copy-done.7, f32[256]{0:T(256)S(1)} %add_rsqrt_fusion), kind=kOutput, calls=%fused_computation.8 | convolution fusion | flops 4299161600 | bytes 18883584 | tf_op jit(solution)/shard_map/dot_general | solution.py:118
  527.0 23.1 %reduce-scatter.5.cloned.1.call-done = bf16[256,512]{1,0:T(8,128)(2,1)} async-done(((bf16[256,2048]{1,0:T(8,128)(2,1)}), bf16[256,512]{1,0:T(8,128)(2,1)}) %reduce-scatter.5.cloned.1.call-update) | async-done | bytes 262160 | tf_op jit(solution)/shard_map/reduce_scatter | solution.py:123
  550.1 1.7 add_convert_fusion
  (125 shorter events, 6.7 us)
Async XLA Ops:
  6.5 72.0 %copy-start = (bf16[4,128,128]{2,1,0:T(8,128)(2,1)S(1)}, bf16[4,128,128]{2,1,0:T(8,128)(2,1)}, u32[]{:S(2)}) copy-start(bf16[4,128,128]{2,1,0:T(8,128)(2,1)} %param.19) | copy-start | bytes 393220
  6.5 69.1 %copy-start.6 = (f32[2048]{0:T(1024)S(1)}, f32[2048]{0:T(1024)}, u32[]{:S(2)}) copy-start(f32[2048]{0:T(1024)} %param.14) | copy-start | bytes 24580
  6.5 21.8 %all-gather.8.cloned.1.call-start = ((), (), s32[]{:S(2)}) async-start(), calls=%async_computation.2 | async-start | bytes 1310720 | tf_op jit(solution)/shard_map/all_gather | solution.py:73
  7.3 68.3 %all-gather.10.cloned.1.call-start = ((), (), s32[]{:S(2)}) async-start(), calls=%async_computation.3 | async-start | bytes 2621440 | tf_op jit(solution)/shard_map/all_gather | solution.py:83
  8.0 113.7 %all-gather.12.cloned.1.call-start = ((), (), s32[]{:S(2)}) async-start(), calls=%async_computation.4 | async-start | bytes 2621440 | tf_op jit(solution)/shard_map/all_gather | solution.py:78
  8.7 158.9 %all-gather.14.cloned.1.call-start = ((), (), s32[]{:S(2)}) async-start(), calls=%async_computation.5 | async-start | bytes 2621440 | tf_op jit(solution)/shard_map/all_gather | solution.py:99
  9.3 186.8 %reduce-scatter.3.cloned.1.call-start = ((), (), s32[]{:S(2)}) async-start(), calls=%async_computation.6 | async-start | bytes 1310720 | tf_op jit(solution)/shard_map/reduce_scatter | solution.py:104
  78.3 0.9 copy-start.5
  78.9 0.8 copy-start.4
  84.9 82.7 %copy-start.3 = (bf16[256,2048]{1,0:T(8,128)(2,1)S(1)}, bf16[256,2048]{1,0:T(8,128)(2,1)}, u32[]{:S(2)}) copy-start(bf16[256,2048]{1,0:T(8,128)(2,1)} %all-gather.8.cloned.1.call-done) | copy-start | bytes 3145732
  85.2 110.9 %copy-start.2 = (bf16[256,512]{1,0:T(8,128)(2,1)S(1)}, bf16[256,512]{1,0:T(8,128)(2,1)}, u32[]{:S(2)}) copy-start(bf16[256,512]{1,0:T(8,128)(2,1)} %param.13) | copy-start | bytes 786436
  172.4 42.3 %all-gather.16.cloned.1.call-start = ((), (), s32[]{:S(2)}) async-start(), calls=%async_computation.7 | async-start | bytes 1310720 | tf_op jit(solution)/shard_map/all_gather | solution.py:108
  197.9 168.1 %all-gather.18.cloned.1.call-start = ((), (), s32[]{:S(2)}) async-start(), calls=%async_computation.8 | async-start | bytes 10485760 | tf_op jit(solution)/shard_map/all_gather | solution.py:113
  198.6 316.7 %copy-start.7 = (f32[2048]{0:T(1024)S(1)}, f32[2048]{0:T(1024)}, u32[]{:S(2)}) copy-start(f32[2048]{0:T(1024)} %param.15) | copy-start | bytes 24580
  198.6 316.7 %all-gather.20.cloned.1.call-start = ((), (), s32[]{:S(2)}) async-start(), calls=%async_computation.9 | async-start | bytes 10485760 | tf_op jit(solution)/shard_map/all_gather | solution.py:120
  199.4 350.7 %reduce-scatter.5.cloned.1.call-start = ((), (), s32[]{:S(2)}) async-start(), calls=%async_computation.10 | async-start | bytes 1310720 | tf_op jit(solution)/shard_map/reduce_scatter | solution.py:123
  216.3 333.8 %copy-start.1 = (bf16[256,512]{1,0:T(8,128)(2,1)S(1)}, bf16[256,512]{1,0:T(8,128)(2,1)}, u32[]{:S(2)}) copy-start(bf16[256,512]{1,0:T(8,128)(2,1)} %add_convert_fusion.1) | copy-start | bytes 786436
Sparse Core Ops, SparseCore 0:
  8.9 19.4 all-gather.7
  29.9 45.6 all-gather.9
  77.2 44.4 all-gather.11
  123.1 44.4 all-gather.13
  172.5 23.5 reduce-scatter.2
  198.0 16.6 all-gather.15
  216.3 149.6 all-gather.17
  367.5 147.7 all-gather.19
  527.1 22.9 reduce-scatter.4
where the time goes:
time: 559 us; the launch traced here: 558 us
  waiting for transfers between devices  511 us (91%)
  matrix products  19.7 us (4%)
  between operations  13.8 us (2%)
  other arithmetic  9.49 us (2%)
    all_gather x1, waiting for transfers between devices, per_device(): lax.all_gather(up_projection_weight, 'fs', axis=0, tiled=True)  150 us
    all_gather x1, waiting for transfers between devices, per_device(): lax.all_gather(down_projection_weight, 'fs', axis=1, tiled=True)  149 us
    all_gather x1, waiting for transfers between devices, per_device(): lax.all_gather(output_projection_weight, 'fs', axis=1, tiled=True)  45.9 us
    all_gather x1, waiting for transfers between devices, per_device(): lax.all_gather(recurrent_projection_weight, 'fs', axis=0, tiled=True)  45.7 us
    all_gather x1, waiting for transfers between devices, per_device(): lax.all_gather(gate_projection_weight, 'fs', axis=0, tiled=True)  36.4 us
    reduce_scatter x1, waiting for transfers between devices, per_device(): lax.psum_scatter(partials.astype(jnp.bfloat16), 'tp', scatter_dimension=1...  23.7 us
    reduce_scatter x1, waiting for transfers between devices, per_device(): lax.psum_scatter(down_terms.astype(jnp.bfloat16), 'tp', scatter_dimension...  23.1 us
    all_gather x1, waiting for transfers between devices, per_device(): whole_rows = lax.all_gather(tokens, 'tp', axis=1, tiled=True)  17.4 us
  transfers between devices with their start and end apart: 9, of which 9 were waited for; matrix products, arithmetic and copies ran while one was open for 2% of the time, Pallas kernels for 0%

commit v1 on v0

--- a/solution.py
+++ b/solution.py
@@ -1,7 +1,26 @@
+import functools
 import jax
 import jax.numpy as jnp
 from jax import lax
 from jax.sharding import PartitionSpec as P
+
+
+def _detail_sample(obj, shard_axis):
+    odd = lax.axis_size(shard_axis)
+    back = lax.axis_index(shard_axis)
+    small, side_arr, step_out = (odd, back, obj.shape[0])
+    item_now, r1 = (obj, 1)
+    while r1 < small:
+        wide_out = lax.ppermute(
+            item_now, shard_axis, perm=[(to_i, (to_i - r1) % small) for to_i in range(small)]
+        )
+        item_now = jnp.concatenate([item_now, wide_out], axis=0)
+        r1 = 2 * r1
+    high = jnp.roll(item_now, side_arr * step_out, axis=0)
+    return high
+
+
+_view_islands = functools.partial(_detail_sample, shard_axis="fs")
 
 
 def rms_rows(values_in, norm_gain):
@@ -74,9 +93,7 @@
     normed = rms_rows(whole_rows, recurrent_norm_gain)
     columns = normed
     gate_pre = jnp.dot(
-        columns,
-        lax.all_gather(gate_projection_weight, "fs", axis=0, tiled=True),
-        preferred_element_type=jnp.float32,
+        columns, _view_islands(gate_projection_weight), preferred_element_type=jnp.float32
     )
     recur_pre = jnp.dot(
         columns,

time: 559 us -> 540 us (0.966)
  waiting for transfers between devices: 511 us -> 481 us
  starting transfers between devices: 0.31 us -> 6.83 us
    ppermute x0 -> x2, waiting for transfers between devices: none -> 89.6 us  [_detail_sample(): lax.ppermute(item_now, shard_axis, perm=[(to_i, (to_i - r1) % small) for...]
    all_gather x1, waiting for transfers between devices: 45.7 us -> 0.02 us  [per_device(): lax.all_gather(recurrent_projection_weight, 'fs', axis=0, tiled=True)]
    all_gather x1 -> x0, waiting for transfers between devices: 36.4 us -> none  [per_device(): lax.all_gather(gate_projection_weight, 'fs', axis=0, tiled=True)]
    all_gather x1, waiting for transfers between devices: 45.9 us -> 27.1 us  [per_device(): lax.all_gather(output_projection_weight, 'fs', axis=1, tiled=True)]
    all_gather x1, waiting for transfers between devices: 17.4 us -> 0.01 us  [per_device(): whole_rows = lax.all_gather(tokens, 'tp', axis=1, tiled=True)]
    ppermute x0 -> x2, starting transfers between devices: none -> 6.55 us  [_detail_sample(): lax.ppermute(item_now, shard_axis, perm=[(to_i, (to_i - r1) % small) for...]
  transfers between devices with their start and end apart: 9 -> 10, of which waited for: 9 -> 8; matrix products, arithmetic and copies ran while one was open for 2% -> 3% of each run, Pallas kernels for 0% -> 0%
where the time goes in v1:
time: 540 us
  waiting for transfers between devices  481 us (89%)
  matrix products  19.7 us (4%)
  between operations  14.2 us (3%)
  local copies, waits for them, and re-layouts  9.66 us (2%)
  other arithmetic  9.12 us (2%)
  starting transfers between devices  6.83 us (1%)
    all_gather x1, waiting for transfers between devices, per_device(): lax.all_gather(up_projection_weight, 'fs', axis=0, tiled=True)  150 us
    all_gather x1, waiting for transfers between devices, per_device(): lax.all_gather(down_projection_weight, 'fs', axis=1, tiled=True)  149 us
    ppermute x2, waiting for transfers between devices, _detail_sample(): lax.ppermute(item_now, shard_axis, perm=[(to_i, (to_i - r1) % small) for...  89.6 us
    all_gather x1, waiting for transfers between devices, per_device(): lax.all_gather(output_projection_weight, 'fs', axis=1, tiled=True)  27.1 us
    reduce_scatter x1, waiting for transfers between devices, per_device(): lax.psum_scatter(partials.astype(jnp.bfloat16), 'tp', scatter_dimension=1...  23.7 us
    reduce_scatter x1, waiting for transfers between devices, per_device(): lax.psum_scatter(down_terms.astype(jnp.bfloat16), 'tp', scatter_dimension...  23.1 us
    all_gather x1, waiting for transfers between devices, per_device(): middle = lax.all_gather(residual, 'tp', axis=1, tiled=True)  15.5 us
    dot_general x1, matrix products, per_device(): jnp.dot(squared, lax.all_gather(down_projection_weight, 'fs', axis=1, til...  11.6 us
  transfers between devices with their start and end apart: 10, of which 8 were waited for; matrix products, arithmetic and copies ran while one was open for 3% of the time, Pallas kernels for 0%

profile of v1, /device:TPU:0, one launch (start us, length us, event | category | flops | bytes accessed | tf_op | source)
XLA Modules:
  0.0 540.1 jit_solution(17931695784055560704)
XLA Ops:
  8.1 5.1 collective-permute-start
  13.2 11.5 %collective-permute-done = bf16[512,512]{1,0:T(8,128)(2,1)S(1)} collective-permute-done((bf16[512,512]{1,0:T(8,128)(2,1)}, bf16[512,512]{1,0:T(8,128)(2,1)S(1)}, u32[]{:S(2)}, u32[]{:S(2)}) %collective-permute-start) | collective-permute-done | bytes 524320 | tf_op jit(solution)/shard_map/ppermute | solution.py:14
  24.7 1.1 pad_maximum_fusion
  25.8 1.4 collective-permute-start.1
  27.3 0.8 constant_dynamic-update-slice_fusion.5
  28.2 0.8 constant_dynamic-update-slice_fusion.4
  29.1 78.1 %collective-permute-done.1 = bf16[1024,512]{1,0:T(8,128)(2,1)S(1)} collective-permute-done((bf16[1024,512]{1,0:T(8,128)(2,1)S(1)}, bf16[1024,512]{1,0:T(8,128)(2,1)S(1)}, u32[]{:S(2)}, u32[]{:S(2)}) %collective-permute-start.1) | collective-permute-done | bytes 1048608 | tf_op jit(solution)/shard_map/ppermute | solution.py:14
  107.2 1.0 constant_dynamic-update-slice_fusion.3
  108.2 0.8 constant_dynamic-update-slice_fusion.2
  109.1 0.8 constant_dynamic-update-slice_fusion.1
  109.9 1.0 constant_dynamic-update-slice_fusion
  110.9 1.5 fusion.2
  112.5 2.7 fusion.16
  122.1 27.1 %all-gather.11.cloned.1.call-done = bf16[512,2048]{1,0:T(8,128)(2,1)} async-done(((bf16[512,512]{1,0:T(8,128)(2,1)}), bf16[512,2048]{1,0:T(8,128)(2,1)}) %all-gather.11.cloned.1.call-update) | async-done | bytes 2097168 | tf_op jit(solution)/shard_map/all_gather | solution.py:116
  149.3 4.7 convolution_convert_fusion
  154.1 23.7 %reduce-scatter.3.cloned.1.call-done = bf16[256,512]{1,0:T(8,128)(2,1)} async-done(((bf16[256,2048]{1,0:T(8,128)(2,1)}), bf16[256,512]{1,0:T(8,128)(2,1)}) %reduce-scatter.3.cloned.1.call-update) | async-done | bytes 262160 | tf_op jit(solution)/shard_map/reduce_scatter | solution.py:121
  177.7 1.7 add_convert_fusion.1
  180.9 15.5 %all-gather.13.cloned.1.call-done = bf16[256,2048]{1,0:T(8,128)(2,1)} async-done(((bf16[256,512]{1,0:T(8,128)(2,1)}), bf16[256,2048]{1,0:T(8,128)(2,1)}) %all-gather.13.cloned.1.call-update) | async-done | bytes 1048592 | tf_op jit(solution)/shard_map/all_gather | solution.py:125
  196.4 1.5 fusion.5
  197.9 149.5 %all-gather.15.cloned.1.call-done = bf16[2048,2048]{1,0:T(8,128)(2,1)} async-done(((bf16[512,2048]{1,0:T(8,128)(2,1)}), bf16[2048,2048]{1,0:T(8,128)(2,1)}) %all-gather.15.cloned.1.call-update) | async-done | bytes 8388624 | tf_op jit(solution)/shard_map/all_gather | solution.py:130
  347.4 149.4 %all-gather.17.cloned.1.call-done = bf16[2048,2048]{1,0:T(8,128)(2,1)} async-done(((bf16[2048,512]{1,0:T(8,128)(2,1)}), bf16[2048,2048]{1,0:T(8,128)(2,1)}) %all-gather.17.cloned.1.call-update) | async-done | bytes 8388624 | tf_op jit(solution)/shard_map/all_gather | solution.py:137
  496.8 11.6 %convolution_convert_fusion.1 = bf16[256,2048]{1,0:T(8,128)(2,1)} fusion(bf16[2048,2048]{1,0:T(8,128)(2,1)} %all-gather.17.cloned.1.call-done, bf16[2048,2048]{1,0:T(8,128)(2,1)} %all-gather.15.cloned.1.call-done, bf16[256,2048]{1,0:T(8,128)(2,1)} %all-gather.13.cloned.1.call-done, f32[2048]{0:T(1024)S(1)} %copy-done.10, f32[256]{0:T(256)S(1)} %add_rsqrt_fusion), kind=kOutput, calls=%fused_computation.8 | convolution fusion | flops 4299161600 | bytes 18883584 | tf_op jit(solution)/shard_map/dot_general | solution.py:135
  508.4 23.1 %reduce-scatter.5.cloned.1.call-done = bf16[256,512]{1,0:T(8,128)(2,1)} async-done(((bf16[256,2048]{1,0:T(8,128)(2,1)}), bf16[256,512]{1,0:T(8,128)(2,1)}) %reduce-scatter.5.cloned.1.call-update) | async-done | bytes 262160 | tf_op jit(solution)/shard_map/reduce_scatter | solution.py:140
  531.5 1.7 add_convert_fusion
  (139 shorter events, 9.4 us)
Async XLA Ops:
  6.5 108.9 %copy-start = (bf16[4,128,128]{2,1,0:T(8,128)(2,1)S(1)}, bf16[4,128,128]{2,1,0:T(8,128)(2,1)}, u32[]{:S(2)}) copy-start(bf16[4,128,128]{2,1,0:T(8,128)(2,1)} %param.19) | copy-start | bytes 393220
  6.5 20.8 %copy-start.1 = (bf16[512,512]{1,0:T(8,128)(2,1)S(1)}, bf16[512,512]{1,0:T(8,128)(2,1)}, u32[]{:S(2)}) copy-start(bf16[512,512]{1,0:T(8,128)(2,1)} %param.16) | copy-start | bytes 1572868
  6.5 104.4 %all-gather.7.cloned.1.call-start = ((), (), s32[]{:S(2)}) async-start(), calls=%async_computation.2 | async-start | bytes 1310720 | tf_op jit(solution)/shard_map/all_gather | solution.py:92
  7.3 20.9 %copy-start.6 = (f32[512]{0:T(512)S(1)}, f32[512]{0:T(512)}, u32[]{:S(2)}) copy-start(f32[512]{0:T(512)} %param.21) | copy-start | bytes 6148
  7.3 20.9 %copy-start.5 = (bf16[4,512]{1,0:T(4,128)(2,1)S(1)}, bf16[4,512]{1,0:T(4,128)(2,1)}, u32[]{:S(2)}) copy-start(bf16[4,512]{1,0:T(4,128)(2,1)} %param.18) | copy-start | bytes 12292
  7.3 105.2 %all-gather.9.cloned.1.call-start = ((), (), s32[]{:S(2)}) async-start(), calls=%async_computation.3 | async-start | bytes 2621440 | tf_op jit(solution)/shard_map/all_gather | solution.py:100
  8.0 141.2 %all-gather.11.cloned.1.call-start = ((), (), s32[]{:S(2)}) async-start(), calls=%async_computation.4 | async-start | bytes 2621440 | tf_op jit(solution)/shard_map/all_gather | solution.py:116
  8.1 16.6 %collective-permute-start = (bf16[512,512]{1,0:T(8,128)(2,1)}, bf16[512,512]{1,0:T(8,128)(2,1)S(1)}, u32[]{:S(2)}, u32[]{:S(2)}) collective-permute-start(bf16[512,512]{1,0:T(8,128)(2,1)} %param.16), channel_id=1, source_target_pairs={{0,12},{4,0},{8,4},{12,8},{1,13},{5,1},{9,5},{13,9},{2,14},{6,2},{... | collective-permute-start | bytes 1572872 | tf_op jit(solution)/shard_map/ppermute | solution.py:14
  25.8 81.4 %collective-permute-start.1 = (bf16[1024,512]{1,0:T(8,128)(2,1)S(1)}, bf16[1024,512]{1,0:T(8,128)(2,1)S(1)}, u32[]{:S(2)}, u32[]{:S(2)}) collective-permute-start(bf16[1024,512]{1,0:T(8,128)(2,1)S(1)} %pad_maximum_fusion), channel_id=1, source_target_pairs={{0,8},{4,12},{8,0},{12,4},{1,9},{5,13},{9,1},{13,5},{2,10},{6,14},... | collective-permute-start | bytes 3145736 | tf_op jit(solution)/shard_map/ppermute | solution.py:14
  27.3 150.5 %reduce-scatter.3.cloned.1.call-start = ((), (), s32[]{:S(2)}) async-start(), calls=%async_computation.5 | async-start | bytes 1310720 | tf_op jit(solution)/shard_map/reduce_scatter | solution.py:121
  109.1 3.5 copy-start.9
  115.2 0.9 copy-start.8
  115.8 0.8 copy-start.7
  121.8 27.5 %copy-start.4 = (bf16[256,2048]{1,0:T(8,128)(2,1)S(1)}, bf16[256,2048]{1,0:T(8,128)(2,1)}, u32[]{:S(2)}) copy-start(bf16[256,2048]{1,0:T(8,128)(2,1)} %all-gather.7.cloned.1.call-done) | copy-start | bytes 3145732
  122.1 55.6 %copy-start.3 = (bf16[256,512]{1,0:T(8,128)(2,1)S(1)}, bf16[256,512]{1,0:T(8,128)(2,1)}, u32[]{:S(2)}) copy-start(bf16[256,512]{1,0:T(8,128)(2,1)} %param.13) | copy-start | bytes 786436
  154.0 42.4 %all-gather.13.cloned.1.call-start = ((), (), s32[]{:S(2)}) async-start(), calls=%async_computation.6 | async-start | bytes 1310720 | tf_op jit(solution)/shard_map/all_gather | solution.py:125
  179.5 167.9 %all-gather.15.cloned.1.call-start = ((), (), s32[]{:S(2)}) async-start(), calls=%async_computation.7 | async-start | bytes 10485760 | tf_op jit(solution)/shard_map/all_gather | solution.py:130
  180.1 316.8 %copy-start.10 = (f32[2048]{0:T(1024)S(1)}, f32[2048]{0:T(1024)}, u32[]{:S(2)}) copy-start(f32[2048]{0:T(1024)} %param.15) | copy-start | bytes 24580
  180.1 316.7 %all-gather.17.cloned.1.call-start = ((), (), s32[]{:S(2)}) async-start(), calls=%async_computation.8 | async-start | bytes 10485760 | tf_op jit(solution)/shard_map/all_gather | solution.py:137
  180.8 350.7 %reduce-scatter.5.cloned.1.call-start = ((), (), s32[]{:S(2)}) async-start(), calls=%async_computation.9 | async-start | bytes 1310720 | tf_op jit(solution)/shard_map/reduce_scatter | solution.py:140
  197.9 333.7 %copy-start.2 = (bf16[256,512]{1,0:T(8,128)(2,1)S(1)}, bf16[256,512]{1,0:T(8,128)(2,1)}, u32[]{:S(2)}) copy-start(bf16[256,512]{1,0:T(8,128)(2,1)} %add_convert_fusion.1) | copy-start | bytes 786436
Sparse Core Ops, SparseCore 0:
  8.9 19.4 all-gather.6
  29.9 73.5 all-gather.8
  105.1 44.1 all-gather.10
  154.1 23.5 reduce-scatter.2
  179.6 16.6 all-gather.12
  197.8 149.6 all-gather.14
  349.0 147.7 all-gather.16
  508.6 22.9 reduce-scatter.4
